TPU v7x, 32 devices: a whole 2x2x4 slice. The times are simulated.
32 devices in a mesh: ep: 4 (over y, x), tp: 8 (over z, core).
Axes of the slice: x: 2, y: 2, z: 4, core: 2. Of those that a mesh axis runs over, the one named last changes fastest.
Arguments:
- residual: bfloat16 [128, 2048], P('ep'), may hold values from -20 to 20
- cache_latent: bfloat16 [128, 2048, 256], P(('ep', 'tp')), may hold values from -12 to 12
- cache_rope: bfloat16 [128, 32, 2048], P(('ep', 'tp')), may hold values from -6 to 6
- lengths: int32 [128], P(('ep', 'tp')), may hold values from 2 to 2048, as said below
- query_latent: bfloat16 [128, 32, 256], P(('ep', 'tp')), may hold values from -250 to 250
- query_rope: bfloat16 [128, 32, 32], P(('ep', 'tp')), may hold values from -6 to 6
- norm_gain: bfloat16 [2048], replicated, may hold values from 0.099609375 to 1.8984375
- latent_weight: bfloat16 [2048, 256], replicated, may hold values from -0.125 to 0.125
- latent_gain: bfloat16 [256], replicated, may hold values from 0.099609375 to 1.8984375
- rope_weight: bfloat16 [32, 2048], replicated, may hold values from -0.125 to 0.125
- value_weight: bfloat16 [256, 2048], replicated, may hold values from -0.375 to 0.375
- out_weight: bfloat16 [2048, 2048], P('tp'), may hold values from -1 to 1
- mixer_gain: bfloat16 [2048], replicated, may hold values from 0.099609375 to 1.8984375
- group_router: bfloat16 [2048, 4], replicated, may hold values from -0.0625 to 0.0625
- expert_router: bfloat16 [2048, 8], replicated, may hold values from -0.0625 to 0.0625
- expert_ids: int32 [128, 2], P('ep'), may hold values from 0 to 7, as said below
- gate_weight: bfloat16 [8, 2048, 4096], P('ep', None, 'tp'), may hold values from -0.125 to 0.125
- up_weight: bfloat16 [8, 2048, 4096], P('ep', None, 'tp'), may hold values from -0.125 to 0.125
- down_weight: bfloat16 [8, 4096, 2048], P('ep', 'tp'), may hold values from -0.75 to 0.75
Outputs:
- mixed: bfloat16 [128, 2048], P('ep')
- new_latent: bfloat16 [128, 256], P(('ep', 'tp'))
- new_rope_key: bfloat16 [128, 32], P(('ep', 'tp'))
Inputs may be any that keep to these rules, and one draw needn't show every extreme that they name: `lengths`: every sequence has 2 or more cached positions, and in every draw some sequence has all 2048. `expert_ids`: each row names 2 different experts of one group; group g holds experts g * 2 to g * 2 + 1. Among the rows of one index of ep (aligned blocks of 32 rows) no expert is named more than 16 times, and in every draw some expert is named exactly 16 times in every block.
All inputs are finite; a program needn't handle non-finite values.
Results may differ from a plain program's by a relative error of at most 0.012.
Values may be sent and summed in bfloat16 or wider, within the bound.
No kernel may reach another device: no remote copies, remote signals or barrier semaphores. Data moves between devices by JAX's collectives and lax.ppermute only.
A program may use at most 64 MiB of HBM per device.

v0:
```python
import jax
import jax.numpy as jnp
from jax import lax
from jax.sharding import PartitionSpec as P

H = 32
KV = 256
ROPE = 32
NOPE = 64
V = 64
GROUPS = 4
TOPK = 2


NORM_EPSILON = 1e-06
ROPE_BASE = 10000.0


def inverse_rms(values):
    return lax.rsqrt(jnp.mean(values * values, axis=-1, keepdims=True) + NORM_EPSILON)


def rotate(vector, position):
    half_width = vector.shape[-1] // 2
    frequency = ROPE_BASE ** (
        -jnp.arange(0, vector.shape[-1], 2, dtype=jnp.float32) / vector.shape[-1]
    )
    angles = position[..., None] * frequency
    lower_half = vector[..., :half_width]
    upper_half = vector[..., half_width:]
    return jnp.concatenate(
        [
            lower_half * jnp.cos(angles) - upper_half * jnp.sin(angles),
            upper_half * jnp.cos(angles) + lower_half * jnp.sin(angles),
        ],
        axis=-1,
    )


def dispatch_table(expert_rows, experts, capacity):
    flat_ids = expert_rows.reshape(-1)
    hit_table = (flat_ids[:, None] == jnp.arange(experts, dtype=jnp.int32)[None, :]).astype(
        jnp.int32
    )
    slot_rank = jnp.sum((jnp.cumsum(hit_table, axis=0) - hit_table) * hit_table, axis=1)
    slot_index = flat_ids * capacity + slot_rank
    picked = (
        slot_index[None, :] == jnp.arange(experts * capacity, dtype=jnp.int32)[:, None]
    ).astype(jnp.float32)
    return picked.reshape(experts * capacity, expert_rows.shape[0], expert_rows.shape[1])


def route_weights(expert_in, group_router, expert_router, expert_ids, per_group):
    group_logits = jnp.dot(expert_in, group_router, preferred_element_type=jnp.float32)
    expert_logits = jnp.dot(expert_in, expert_router, preferred_element_type=jnp.float32)
    chosen = expert_ids[:, 0] // per_group
    group_hit = (
        jnp.arange(group_logits.shape[1], dtype=jnp.int32)[None, :] == chosen[:, None]
    ).astype(jnp.float32)
    chosen_logit = jnp.sum(group_logits * group_hit, axis=1, keepdims=True)
    group_share = 1.0 / jnp.sum(jnp.exp(group_logits - chosen_logit), axis=1)
    expert_hit = (
        expert_ids[:, :, None] == jnp.arange(expert_logits.shape[1], dtype=jnp.int32)[None, None, :]
    ).astype(jnp.float32)
    picked_logit = jnp.sum(expert_hit * expert_logits[:, None, :], axis=2)
    inner_share = 1.0 / jnp.sum(
        jnp.exp(picked_logit[:, None, :] - picked_logit[:, :, None]), axis=2
    )
    return group_share[:, None] * inner_share


def on_device(
    residual,
    cache_latent,
    cache_rope,
    lengths,
    query_latent,
    query_rope,
    norm_gain,
    latent_weight,
    latent_gain,
    rope_weight,
    value_weight,
    out_weight,
    mixer_gain,
    group_router,
    expert_router,
    expert_ids,
    gate_weight,
    up_weight,
    down_weight,
):
    ep_count = lax.axis_size("ep")
    seq_count = cache_latent.shape[0]
    group_rows = residual.shape[0]
    model_width = residual.shape[1]
    resid_f = residual.astype(jnp.float32)
    own_rows = lax.dynamic_slice_in_dim(resid_f, lax.axis_index("tp") * seq_count, seq_count, 0)
    normed = (own_rows * inverse_rms(own_rows) * norm_gain.astype(jnp.float32)).astype(jnp.bfloat16)
    latent_raw = jnp.dot(normed, latent_weight, preferred_element_type=jnp.float32)
    new_latent = (latent_raw * inverse_rms(latent_raw) * latent_gain.astype(jnp.float32)).astype(
        jnp.bfloat16
    )
    positions = lengths.astype(jnp.float32)
    rope_raw = jnp.dot(normed, rope_weight.T, preferred_element_type=jnp.float32)
    new_rope_key = rotate(rope_raw, positions).astype(jnp.bfloat16)
    query_turned = rotate(query_rope.astype(jnp.float32), positions[:, None]).astype(jnp.bfloat16)
    score_scale = (NOPE + ROPE) ** (-0.5)
    cached = (
        jnp.einsum("shc,spc->shp", query_latent, cache_latent, preferred_element_type=jnp.float32)
        + jnp.einsum("shr,srp->shp", query_turned, cache_rope, preferred_element_type=jnp.float32)
    ) * score_scale
    keeping = (
        jnp.arange(cache_latent.shape[1], dtype=jnp.int32)[None, None, :] < lengths[:, None, None]
    )
    cached = jnp.where(keeping, cached, -jnp.inf)
    fresh = (
        jnp.einsum("shc,sc->sh", query_latent, new_latent, preferred_element_type=jnp.float32)
        + jnp.einsum("shr,sr->sh", query_turned, new_rope_key, preferred_element_type=jnp.float32)
    ) * score_scale
    row_top = jnp.maximum(jnp.max(cached, axis=2), fresh)
    cached_exp = jnp.exp(cached - row_top[:, :, None])
    fresh_exp = jnp.exp(fresh - row_top)
    denominator = jnp.sum(cached_exp, axis=2) + fresh_exp
    cached_weight = (cached_exp / denominator[:, :, None]).astype(jnp.bfloat16)
    fresh_weight = (fresh_exp / denominator).astype(jnp.bfloat16)
    mixed_latent = (
        jnp.einsum("shp,spc->shc", cached_weight, cache_latent, preferred_element_type=jnp.float32)
        + fresh_weight.astype(jnp.float32)[:, :, None] * new_latent.astype(jnp.float32)[:, None, :]
    ).astype(jnp.bfloat16)
    head_values = jnp.einsum(
        "shc,chv->shv",
        mixed_latent,
        value_weight.reshape(KV, H, V),
        preferred_element_type=jnp.float32,
    ).astype(jnp.bfloat16)
    by_heads = lax.all_to_all(head_values, "tp", split_axis=1, concat_axis=0, tiled=True)
    head_terms = jnp.dot(
        by_heads.reshape(group_rows, -1), out_weight, preferred_element_type=jnp.float32
    )
    attended = lax.psum(head_terms, "tp")
    after_attention = (resid_f + attended).astype(jnp.bfloat16)
    after_f = after_attention.astype(jnp.float32)
    expert_in = (after_f * inverse_rms(after_f) * mixer_gain.astype(jnp.float32)).astype(
        jnp.bfloat16
    )
    experts = expert_router.shape[1]
    capacity = 2 * group_rows * TOPK // experts
    route_weight = route_weights(
        expert_in, group_router, expert_router, expert_ids, experts // GROUPS
    )
    picked = dispatch_table(expert_ids, experts, capacity)
    select_rows = jnp.sum(picked, axis=2).astype(jnp.bfloat16)
    outbound = jnp.dot(select_rows, expert_in, preferred_element_type=jnp.float32).astype(
        jnp.bfloat16
    )
    outbound = outbound.reshape(ep_count, gate_weight.shape[0], capacity, model_width)
    rows = lax.all_to_all(outbound, "ep", split_axis=0, concat_axis=0, tiled=True)
    gate_value = jnp.einsum("secd,edf->secf", rows, gate_weight, preferred_element_type=jnp.float32)
    up_value = jnp.einsum("secd,edf->secf", rows, up_weight, preferred_element_type=jnp.float32)
    activation = (jax.nn.silu(gate_value) * up_value).astype(jnp.bfloat16)
    expert_terms = jnp.einsum(
        "secf,efd->secd", activation, down_weight, preferred_element_type=jnp.float32
    )
    combine = jnp.sum(picked * route_weight[None, :, :], axis=2).T
    summed_terms = lax.psum_scatter(expert_terms, "tp", scatter_dimension=3, tiled=True)
    returned_terms = lax.all_to_all(summed_terms, "ep", split_axis=0, concat_axis=0, tiled=True)
    share_width = returned_terms.shape[3]
    moe_part = jnp.dot(
        combine, returned_terms.reshape(-1, share_width), precision=lax.Precision.HIGHEST
    )
    after_cols = lax.dynamic_slice_in_dim(
        after_f, lax.axis_index("tp") * share_width, share_width, 1
    )
    mixed_share = (after_cols + moe_part).astype(jnp.bfloat16)
    mixed = lax.all_gather(mixed_share, "tp", axis=1, tiled=True)
    return (mixed, new_latent, new_rope_key)


def solution(mesh):
    in_specs = (
        P("ep", None),
        P(("ep", "tp"), None, None),
        P(("ep", "tp"), None, None),
        P(("ep", "tp")),
        P(("ep", "tp"), None, None),
        P(("ep", "tp"), None, None),
        P(),
        P(),
        P(),
        P(),
        P(),
        P("tp", None),
        P(),
        P(),
        P(),
        P("ep", None),
        P("ep", None, "tp"),
        P("ep", None, "tp"),
        P("ep", "tp", None),
    )
    out_specs = (P("ep", None), P(("ep", "tp"), None), P(("ep", "tp"), None))
    return jax.shard_map(
        on_device, mesh=mesh, in_specs=in_specs, out_specs=out_specs, check_vma=False
    )
```

profile of v0, /device:TPU:0, one launch (start us, length us, event | category | flops | bytes accessed | tf_op | source)
XLA Modules:
  0.0 177.1 jit_solution(6395437696958432695)
XLA Ops:
  7.2 0.8 convert_element_type.79
  8.0 0.7 iota_compare_fusion.2
  8.7 0.9 convert_element_type.77
  9.8 0.7 convert_element_type.80
  10.5 0.8 convert_element_type.78
  11.3 1.1 fusion.50
  12.4 1.6 multiply_reduce_fusion.2
  14.7 3.5 %fusion.58 = f32[4,32,2048]{2,1,0:T(8,128)S(1)} fusion(bf16[4,32,256]{2,1,0:T(8,128)(2,1)} %param.23, bf16[4,2048,256]{2,1,0:T(8,128)(2,1)} %param.20), kind=kOutput, calls=%fused_computation.90 | convolution fusion | flops 134217728 | bytes 5308416 | tf_op jit(solution)/shard_map/shc,spc->shp/dot_general | solution.py:110
  19.8 1.5 copy.61
  21.3 3.1 %fusion.23 = bf16[4,32,256]{2,1,0:T(8,128)(2,1)S(1)} fusion(bf16[4,2048,256]{2,1,0:T(8,128)(2,1)} %param.20, f32[4,32,2048]{2,1,0:T(8,128)S(1)} %get-tuple-element.18, f32[4,32]{1,0:T(4,128)S(1)} %get-tuple-element.12, f32[4,32]{1,0:T(4,128)S(1)} %fusion.44, f32[4,256]{1,0:T(4,128)S(1)} %get-tuple-element.7, f32[4,32]{1,0:T(4,128)S(1)} %get-tuple-element.11), kind=kOutput, calls=%fused_computation.16 | convolution fusion | flops 135102464 | bytes 5314048 | tf_op jit(solution)/shard_map/shp,spc->shc/dot_general | solution.py:128
  24.8 0.7 reshape.194
  25.5 6.4 %all-to-all-start = ((bf16[8,2,512]{2,1,0:T(2,128)(2,1)}), bf16[8,2,512]{2,1,0:T(2,128)(2,1)S(1)}, u32[]{:S(2)}, u32[]{:S(2)}) async-start(bf16[8,2,512]{2,1,0:T(2,128)(2,1)} %reshape.194), calls=%async_computation | async-start | bytes 32768 | tf_op jit(solution)/shard_map/all_to_all | solution.py:137
  32.7 4.8 %all-to-all-done = bf16[8,2,512]{2,1,0:T(2,128)(2,1)S(1)} async-done(((bf16[8,2,512]{2,1,0:T(2,128)(2,1)}), bf16[8,2,512]{2,1,0:T(2,128)(2,1)S(1)}, u32[]{:S(2)}, u32[]{:S(2)}) %all-to-all-start) | async-done | bytes 16416 | tf_op jit(solution)/shard_map/all_to_all | solution.py:137
  37.7 1.0 fusion.59
  38.8 53.8 %all-reduce.2.cloned.1.call-done = f32[32,2048]{1,0:T(8,128)} async-done(((f32[32,2048]{1,0:T(8,128)}), f32[32,2048]{1,0:T(8,128)}) %all-reduce.2.cloned.1.call-update) | async-done | bytes 262160 | tf_op jit(solution)/shard_map/psum | solution.py:141
  92.6 1.1 multiply_reduce_fusion
  94.6 10.6 %all_to_all.25 = bf16[4,2,16,2048]{3,2,1,0:T(8,128)(2,1)S(1)} all-to-all(bf16[4,2,16,2048]{3,2,1,0:T(8,128)(2,1)S(1)} %bitcast.81), channel_id=1, replica_groups=mesh['ep'=4,'tp'=8] {'ep'}, dimensions={0} | all-to-all | bytes 1048576 | tf_op jit(solution)/shard_map/all_to_all | solution.py:158
  105.2 3.0 %fusion.11 = f32[4,2,16,512]{3,2,0,1:T(8,128)S(1)} fusion(bf16[2,2048,512]{2,1,0:T(8,128)(2,1)} %param.35, bf16[4,2,16,2048]{3,2,1,0:T(8,128)(2,1)S(1)} %all_to_all.25), kind=kOutput, calls=%fused_computation.11 | convolution fusion | flops 268435456 | bytes 4980736 | tf_op jit(solution)/shard_map/secd,edf->secf/dot_general | solution.py:159
  108.2 6.0 %fusion.6 = f32[4,2,16,2048]{3,2,0,1:T(8,128)} fusion(bf16[2,512,2048]{2,1,0:T(8,128)(2,1)} %param.37, bf16[2,2048,512]{2,1,0:T(8,128)(2,1)} %param.36, bf16[4,2,16,2048]{3,2,1,0:T(8,128)(2,1)S(1)} %all_to_all.25, f32[4,2,16,512]{3,2,0,1:T(8,128)S(1)} %fusion.11), kind=kOutput, calls=%fused_computation.6 | convolution fusion | flops 537264128 | bytes 10223616 | tf_op jit(solution)/shard_map/secf,efd->secd/dot_general | solution.py:162
  114.3 30.9 %reduce-scatter.2.cloned.1.call-done = f32[4,2,16,256]{3,2,0,1:T(8,128)} async-done(((f32[4,2,16,2048]{3,2,0,1:T(8,128)}), f32[4,2,16,256]{3,2,0,1:T(8,128)}) %reduce-scatter.2.cloned.1.call-update) | async-done | bytes 131088 | tf_op jit(solution)/shard_map/reduce_scatter | solution.py:166
  145.2 1.6 copy.68
  146.8 3.7 %all-to-all-start.2 = ((f32[4,2,16,256]{3,2,1,0:T(8,128)}), f32[4,2,16,256]{3,2,1,0:T(8,128)S(1)}, u32[]{:S(2)}, u32[]{:S(2)}) async-start(f32[4,2,16,256]{3,2,1,0:T(8,128)} %copy.68), calls=%async_computation.3 | async-start | bytes 262144 | tf_op jit(solution)/shard_map/all_to_all | solution.py:167
  151.1 4.4 %all-to-all-done.2 = f32[4,2,16,256]{3,2,1,0:T(8,128)S(1)} async-done(((f32[4,2,16,256]{3,2,1,0:T(8,128)}), f32[4,2,16,256]{3,2,1,0:T(8,128)S(1)}, u32[]{:S(2)}, u32[]{:S(2)}) %all-to-all-start.2) | async-done | bytes 131104 | tf_op jit(solution)/shard_map/all_to_all | solution.py:167
  155.6 14.0 %all_gather.3 = bf16[32,2048]{1,0:T(8,128)(2,1)S(1)} all-gather(bf16[32,256]{1,0:T(8,128)(2,1)S(1)} %fusion.25), channel_id=1, replica_groups=mesh['ep'=4,'tp'=8] {'tp'}, dimensions={1}, use_global_device_ids=true | all-gather | bytes 147456 | tf_op jit(solution)/shard_map/all_gather | solution.py:176
  (65 shorter events, 6.2 us)
Async XLA Ops:
  7.2 30.6 %copy-start = (bf16[256,2048]{1,0:T(8,128)(2,1)S(1)}, bf16[256,2048]{1,0:T(8,128)(2,1)}, u32[]{:S(2)}) copy-start(bf16[256,2048]{1,0:T(8,128)(2,1)} %param.30) | copy-start | bytes 3145732
  7.2 11.1 %copy-start.3 = (bf16[4,32,256]{2,1,0:T(8,128)(2,1)S(1)}, bf16[4,32,256]{2,1,0:T(8,128)(2,1)}, u32[]{:S(2)}) copy-start(bf16[4,32,256]{2,1,0:T(8,128)(2,1)} %param.23) | copy-start | bytes 196612
  7.2 11.7 %copy-start.2 = (bf16[4,32,2048]{2,1,0:T(8,128)(2,1)S(1)}, bf16[4,32,2048]{2,1,0:T(8,128)(2,1)}, u32[]{:S(2)}) copy-start(bf16[4,32,2048]{2,1,0:T(8,128)(2,1)} %param.21) | copy-start | bytes 1572868
  18.3 6.1 %copy-start.7 = (bf16[4,256]{1,0:T(4,128)(2,1)}, bf16[4,256]{1,0:T(4,128)(2,1)S(1)}, u32[]{:S(2)}) copy-start(bf16[4,256]{1,0:T(4,128)(2,1)S(1)} %get-tuple-element.27) | copy-start | bytes 6148
  21.2 10.7 %copy-start.5 = (s32[32,2]{0,1:T(2,128)S(1)}, s32[32,2]{0,1:T(2,128)}, u32[]{:S(2)}) copy-start(s32[32,2]{0,1:T(2,128)} %param.34) | copy-start | bytes 772
  21.3 11.4 %copy-start.6 = (bf16[2048]{0:T(1024)(128)(2,1)S(1)}, bf16[2048]{0:T(1024)(128)(2,1)}, u32[]{:S(2)}) copy-start(bf16[2048]{0:T(1024)(128)(2,1)} %param.31) | copy-start | bytes 12292
  21.3 71.3 %copy-start.1 = (bf16[32,2048]{1,0:T(8,128)(2,1)S(1)}, bf16[32,2048]{1,0:T(8,128)(2,1)}, u32[]{:S(2)}) copy-start(bf16[32,2048]{1,0:T(8,128)(2,1)} %param.19) | copy-start | bytes 393220
  21.3 72.5 %copy-start.8 = (bf16[2048,4]{0,1:T(4,128)(2,1)S(1)}, bf16[2048,4]{0,1:T(4,128)(2,1)}, u32[]{:S(2)}) copy-start(bf16[2048,4]{0,1:T(4,128)(2,1)} %param.32) | copy-start | bytes 49156
  21.3 72.7 %copy-start.4 = (bf16[2048,8]{0,1:T(8,128)(2,1)S(1)}, bf16[2048,8]{0,1:T(8,128)(2,1)}, u32[]{:S(2)}) copy-start(bf16[2048,8]{0,1:T(8,128)(2,1)} %param.33) | copy-start | bytes 98308
  25.5 12.0 %all-to-all-start = ((bf16[8,2,512]{2,1,0:T(2,128)(2,1)}), bf16[8,2,512]{2,1,0:T(2,128)(2,1)S(1)}, u32[]{:S(2)}, u32[]{:S(2)}) async-start(bf16[8,2,512]{2,1,0:T(2,128)(2,1)} %reshape.194), calls=%async_computation | async-start | bytes 32768 | tf_op jit(solution)/shard_map/all_to_all | solution.py:137
  31.9 60.7 %all-reduce.2.cloned.1.call-start = ((), (), s32[]{:S(2)}) async-start(), calls=%async_computation.4 | async-start | bytes 524288 | tf_op jit(solution)/shard_map/psum | solution.py:141
  38.7 106.5 %reduce-scatter.2.cloned.1.call-start = ((), (), s32[]{:S(2)}) async-start(), calls=%async_computation.5 | async-start | bytes 1179648 | tf_op jit(solution)/shard_map/reduce_scatter | solution.py:166
  146.8 8.7 %all-to-all-start.2 = ((f32[4,2,16,256]{3,2,1,0:T(8,128)}), f32[4,2,16,256]{3,2,1,0:T(8,128)S(1)}, u32[]{:S(2)}, u32[]{:S(2)}) async-start(f32[4,2,16,256]{3,2,1,0:T(8,128)} %copy.68), calls=%async_computation.3 | async-start | bytes 262144 | tf_op jit(solution)/shard_map/all_to_all | solution.py:167
Sparse Core Ops, SparseCore 0:
  38.9 53.6 all-reduce.1
  114.4 30.7 reduce-scatter.1
where the time goes:
time: 178 us; the launch traced here: 177 us
  waiting for transfers between devices  93.9 us (53%)
  blocking collectives  24.5 us (14%)
  matrix products  21.4 us (12%)
  between operations  14.3 us (8%)
  starting transfers between devices  10.1 us (6%)
  other arithmetic  7.81 us (4%)
  local copies, waits for them, and re-layouts  5.06 us (3%)
    psum x1, waiting for transfers between devices, on_device(): attended = lax.psum(head_terms, 'tp')  53.8 us
    reduce_scatter x1, waiting for transfers between devices, on_device(): lax.psum_scatter(expert_terms, 'tp', scatter_dimension=3, tiled=True)  30.9 us
    all_gather x1, blocking collectives, on_device(): mixed = lax.all_gather(mixed_share, 'tp', axis=1, tiled=True)  14 us
    all_to_all x1, blocking collectives, on_device(): lax.all_to_all(outbound, 'ep', split_axis=0, concat_axis=0, tiled=True)  10.6 us
    all_to_all x1, starting transfers between devices, on_device(): lax.all_to_all(head_values, 'tp', split_axis=1, concat_axis=0, tiled=True)  6.35 us
    dot_general x1, matrix products, on_device(): jnp.einsum('secf,efd->secd', activation, down_weight, preferred_element_t...  6.04 us
    all_to_all x1, waiting for transfers between devices, on_device(): lax.all_to_all(head_values, 'tp', split_axis=1, concat_axis=0, tiled=True)  4.83 us
    all_to_all x1, waiting for transfers between devices, on_device(): lax.all_to_all(summed_terms, 'ep', split_axis=0, concat_axis=0, tiled=True)  4.38 us
  transfers between devices with their start and end apart: 4, of which 4 were waited for; matrix products, arithmetic and copies ran while one was open for 1% of the time, Pallas kernels for 0%

commit v1 on v0

--- a/solution.py
+++ b/solution.py
@@ -37,17 +37,23 @@
     )
 
 
-def dispatch_table(expert_rows, experts, capacity):
-    flat_ids = expert_rows.reshape(-1)
-    hit_table = (flat_ids[:, None] == jnp.arange(experts, dtype=jnp.int32)[None, :]).astype(
-        jnp.int32
-    )
-    slot_rank = jnp.sum((jnp.cumsum(hit_table, axis=0) - hit_table) * hit_table, axis=1)
-    slot_index = flat_ids * capacity + slot_rank
-    picked = (
-        slot_index[None, :] == jnp.arange(experts * capacity, dtype=jnp.int32)[:, None]
-    ).astype(jnp.float32)
-    return picked.reshape(experts * capacity, expert_rows.shape[0], expert_rows.shape[1])
+def slot_table(expert_ids, ep_count, local_experts, slots):
+    hits = jnp.any(
+        (expert_ids // local_experts)[:, :, None]
+        == jnp.arange(ep_count, dtype=jnp.int32)[None, None, :],
+        axis=1,
+    )
+    row = jnp.arange(expert_ids.shape[0], dtype=jnp.int32)
+    earlier = (row[None, :] < row[:, None]).astype(jnp.float32)
+    rank = jnp.dot(earlier, hits.astype(jnp.float32))
+    slot = jnp.arange(slots, dtype=jnp.float32)
+    picked = (rank.T[:, None, :] == slot[None, :, None]) & hits.T[:, None, :]
+    return picked.astype(jnp.float32)
+
+
+def gather_copies(block, axis):
+    copies = jnp.broadcast_to(block[None], (lax.axis_size(axis),) + block.shape)
+    return lax.all_to_all(copies, axis, split_axis=0, concat_axis=0, tiled=True)
 
 
 def route_weights(expert_in, group_router, expert_router, expert_ids, per_group):
@@ -134,46 +140,83 @@
         value_weight.reshape(KV, H, V),
         preferred_element_type=jnp.float32,
     ).astype(jnp.bfloat16)
-    by_heads = lax.all_to_all(head_values, "tp", split_axis=1, concat_axis=0, tiled=True)
-    head_terms = jnp.dot(
-        by_heads.reshape(group_rows, -1), out_weight, preferred_element_type=jnp.float32
-    )
-    attended = lax.psum(head_terms, "tp")
-    after_attention = (resid_f + attended).astype(jnp.bfloat16)
-    after_f = after_attention.astype(jnp.float32)
-    expert_in = (after_f * inverse_rms(after_f) * mixer_gain.astype(jnp.float32)).astype(
-        jnp.bfloat16
-    )
+    tp_count = lax.axis_size("tp")
+    share_width = model_width // tp_count
     experts = expert_router.shape[1]
+    per_group = experts // GROUPS
+    local_experts = gate_weight.shape[0]
     capacity = 2 * group_rows * TOPK // experts
-    route_weight = route_weights(
-        expert_in, group_router, expert_router, expert_ids, experts // GROUPS
-    )
-    picked = dispatch_table(expert_ids, experts, capacity)
-    select_rows = jnp.sum(picked, axis=2).astype(jnp.bfloat16)
-    outbound = jnp.dot(select_rows, expert_in, preferred_element_type=jnp.float32).astype(
-        jnp.bfloat16
-    )
-    outbound = outbound.reshape(ep_count, gate_weight.shape[0], capacity, model_width)
-    rows = lax.all_to_all(outbound, "ep", split_axis=0, concat_axis=0, tiled=True)
-    gate_value = jnp.einsum("secd,edf->secf", rows, gate_weight, preferred_element_type=jnp.float32)
-    up_value = jnp.einsum("secd,edf->secf", rows, up_weight, preferred_element_type=jnp.float32)
+    whole_groups = per_group == TOPK and local_experts == TOPK
+    slots = capacity if whole_groups else capacity * local_experts
+    first_column = lax.axis_index("tp") * share_width
+    first_expert = lax.axis_index("ep") * local_experts
+
+    heads = gather_copies(head_values.reshape(seq_count, -1), "tp").reshape(group_rows, -1)
+    out_columns = lax.all_to_all(out_weight, "tp", split_axis=1, concat_axis=0, tiled=True)
+    attended = jnp.dot(heads, out_columns, preferred_element_type=jnp.float32)
+    resid_columns = lax.dynamic_slice_in_dim(residual, first_column, share_width, 1)
+    after_columns = (resid_columns.astype(jnp.float32) + attended).astype(jnp.bfloat16)
+
+    sel = slot_table(expert_ids, ep_count, local_experts, slots)
+    if whole_groups:
+        slot_ids = first_expert + jnp.broadcast_to(
+            jnp.arange(TOPK, dtype=jnp.int32)[None], (ep_count * slots, TOPK)
+        )
+    else:
+        all_ids = lax.all_gather(expert_ids, "ep")
+        all_sel = jax.vmap(lambda ids: slot_table(ids, ep_count, local_experts, slots))(all_ids)
+        mine = lax.dynamic_index_in_dim(all_sel, lax.axis_index("ep"), 1, keepdims=False)
+        slot_ids = jnp.einsum(
+            "esr,erk->esk", mine, all_ids.astype(jnp.float32), precision=lax.Precision.HIGHEST
+        )
+        slot_ids = slot_ids.astype(jnp.int32).reshape(-1, TOPK)
+    sent = jnp.dot(
+        sel.reshape(-1, group_rows).astype(jnp.bfloat16),
+        after_columns,
+        preferred_element_type=jnp.float32,
+    ).astype(jnp.bfloat16)
+    sent = jnp.broadcast_to(
+        sent.reshape(ep_count, 1, slots, share_width), (ep_count, tp_count, slots, share_width)
+    )
+    came = lax.all_to_all(
+        sent.reshape(-1, slots, share_width), ("ep", "tp"), split_axis=0, concat_axis=0, tiled=True
+    )
+    rows_f = (
+        came.reshape(ep_count, tp_count, slots, share_width)
+        .transpose(0, 2, 1, 3)
+        .reshape(-1, model_width)
+        .astype(jnp.float32)
+    )
+    expert_in = (rows_f * inverse_rms(rows_f) * mixer_gain.astype(jnp.float32)).astype(jnp.bfloat16)
+    route_weight = route_weights(expert_in, group_router, expert_router, slot_ids, per_group)
+    local = first_expert + jnp.arange(local_experts, dtype=jnp.int32)
+    row_weight = jnp.sum(
+        (slot_ids[:, :, None] == local[None, None, :]) * route_weight[:, :, None], axis=1
+    )
+    gate_value = jnp.einsum("rd,edf->erf", expert_in, gate_weight, preferred_element_type=jnp.float32)
+    up_value = jnp.einsum("rd,edf->erf", expert_in, up_weight, preferred_element_type=jnp.float32)
     activation = (jax.nn.silu(gate_value) * up_value).astype(jnp.bfloat16)
     expert_terms = jnp.einsum(
-        "secf,efd->secd", activation, down_weight, preferred_element_type=jnp.float32
-    )
-    combine = jnp.sum(picked * route_weight[None, :, :], axis=2).T
-    summed_terms = lax.psum_scatter(expert_terms, "tp", scatter_dimension=3, tiled=True)
-    returned_terms = lax.all_to_all(summed_terms, "ep", split_axis=0, concat_axis=0, tiled=True)
-    share_width = returned_terms.shape[3]
+        "erf,efd->erd", activation, down_weight, preferred_element_type=jnp.float32
+    )
+    row_terms = jnp.sum(expert_terms * row_weight.T[:, :, None], axis=0).astype(jnp.bfloat16)
+    back = lax.all_to_all(
+        row_terms.reshape(ep_count, slots, tp_count, share_width)
+        .transpose(0, 2, 1, 3)
+        .reshape(-1, slots, share_width),
+        ("ep", "tp"),
+        split_axis=0,
+        concat_axis=0,
+        tiled=True,
+    )
+    slot_sums = jnp.sum(
+        back.reshape(ep_count, tp_count, slots, share_width).astype(jnp.float32), axis=1
+    ).reshape(-1, share_width)
     moe_part = jnp.dot(
-        combine, returned_terms.reshape(-1, share_width), precision=lax.Precision.HIGHEST
-    )
-    after_cols = lax.dynamic_slice_in_dim(
-        after_f, lax.axis_index("tp") * share_width, share_width, 1
-    )
-    mixed_share = (after_cols + moe_part).astype(jnp.bfloat16)
-    mixed = lax.all_gather(mixed_share, "tp", axis=1, tiled=True)
+        sel.reshape(-1, group_rows).T, slot_sums, precision=lax.Precision.HIGHEST
+    )
+    mixed_share = (after_columns.astype(jnp.float32) + moe_part).astype(jnp.bfloat16)
+    mixed = gather_copies(mixed_share, "tp").transpose(1, 0, 2).reshape(group_rows, model_width)
     return (mixed, new_latent, new_rope_key)
 
 

time: 178 us -> 112 us (0.63)
  waiting for transfers between devices: 93.9 us -> 46.4 us
  between operations: 14.3 us -> 1.17 us
  blocking collectives: 24.5 us -> 12.7 us
  starting transfers between devices: 10.1 us -> 16.8 us
  local copies, waits for them, and re-layouts: 5.06 us -> 8 us
    psum x1 -> x0, waiting for transfers between devices: 53.8 us -> none  [on_device(): attended = lax.psum(head_terms, 'tp')]
    all_to_all x2 -> x4, waiting for transfers between devices: 9.22 us -> 46.4 us  [the longest x1 26.1 us: on_device(): lax.all_to_all(out_weight, 'tp', split_axis=1, concat_axis=0, tiled=True)]
    reduce_scatter x1 -> x0, waiting for transfers between devices: 30.9 us -> none  [on_device(): lax.psum_scatter(expert_terms, 'tp', scatter_dimension=3, tiled=True)]
    all_gather x1 -> x0, blocking collectives: 14 us -> none  [on_device(): mixed = lax.all_gather(mixed_share, 'tp', axis=1, tiled=True)]
    all_to_all x2 -> x4, starting transfers between devices: 10 us -> 16.8 us  [the longest x2 9.73 us: gather_copies(): return lax.all_to_all(copies, axis, split_axis=0, concat_axis=0, tiled=True)]
    broadcast_in_dim x0 -> x4, local copies, waits for them, and re-layouts: none -> 2.18 us  [the longest x3 1.46 us: gather_copies(): copies = jnp.broadcast_to(block[None], (lax.axis_size(axis),) + block.shape)]
    all_to_all x1, blocking collectives: 10.6 us -> 12.7 us  [on_device(): lax.all_to_all(row_terms.reshape(ep_count, slots, tp_count, share_width)....]
    dot_general x5 -> x6, matrix products: 10.5 us -> 9.51 us  [the longest x1 5.05 us: on_device(): jnp.einsum('erf,efd->erd', activation, down_weight, preferred_element_typ...]
  transfers between devices with their start and end apart: 4 -> 4, of which waited for: 4 -> 4; matrix products, arithmetic and copies ran while one was open for 1% -> 3% of each run, Pallas kernels for 0% -> 0%
where the time goes in v1:
time: 112 us
  waiting for transfers between devices  46.4 us (41%)
  matrix products  19.9 us (18%)
  starting transfers between devices  16.8 us (15%)
  blocking collectives  12.7 us (11%)
  local copies, waits for them, and re-layouts  8 us (7%)
  other arithmetic  6.62 us (6%)
  between operations  1.17 us (1%)
    all_to_all x1, waiting for transfers between devices, on_device(): lax.all_to_all(out_weight, 'tp', split_axis=1, concat_axis=0, tiled=True)  26.1 us
    all_to_all x1, blocking collectives, on_device(): lax.all_to_all(row_terms.reshape(ep_count, slots, tp_count, share_width)....  12.7 us
    all_to_all x2, waiting for transfers between devices, gather_copies(): return lax.all_to_all(copies, axis, split_axis=0, concat_axis=0, tiled=True)  10.5 us
    all_to_all x1, waiting for transfers between devices, on_device(): lax.all_to_all(sent.reshape(-1, slots, share_width), ('ep', 'tp'), split_...  9.8 us
    all_to_all x2, starting transfers between devices, gather_copies(): return lax.all_to_all(copies, axis, split_axis=0, concat_axis=0, tiled=True)  9.73 us
    dot_general x1, matrix products, on_device(): jnp.einsum('erf,efd->erd', activation, down_weight, preferred_element_typ...  5.05 us
    unnamed x20, local copies, waits for them, and re-layouts  4.03 us
    all_to_all x1, starting transfers between devices, on_device(): lax.all_to_all(out_weight, 'tp', split_axis=1, concat_axis=0, tiled=True)  3.56 us
  transfers between devices with their start and end apart: 4, of which 4 were waited for; matrix products, arithmetic and copies ran while one was open for 3% of the time, Pallas kernels for 0%

profile of v1, /device:TPU:0, one launch (start us, length us, event | category | flops | bytes accessed | tf_op | source)
XLA Modules:
  0.0 111.5 jit_solution(3287054261069369241)
XLA Ops:
  0.7 0.8 convert_element_type.112
  1.5 0.7 iota_compare_fusion.1
  2.2 0.9 fusion.25
  3.8 0.8 convert_element_type.111
  4.6 1.1 %fusion.44 = f32[4,32]{1,0:T(4,128)S(1)} fusion(bf16[32,2048]{1,0:T(8,128)(2,1)} %param.28, f32[2048]{0:T(1024)S(1)} %convert_element_type.114, f32[4]{0:T(128)S(1)} %add_rsqrt_fusion.2, bf16[32,2048]{1,0:T(8,128)(2,1)} %param.19, s32[]{:T(128)S(6)} %select_n.26), kind=kOutput, calls=%fused_computation.97 | convolution fusion | flops 557056 | bytes 156180 | tf_op jit(solution)/shard_map/dot_general | solution.py:111
  5.7 1.2 %multiply_reduce_fusion.1 = (f32[4]{0:T(128)S(1)}, f32[4,256]{1,0:T(4,128)S(1)}) fusion(bf16[2048,256]{1,0:T(8,128)(2,1)S(1)} %copy-done, f32[2048]{0:T(1024)S(1)} %convert_element_type.114, f32[4]{0:T(128)S(1)} %add_rsqrt_fusion.2, bf16[32,2048]{1,0:T(8,128)(2,1)} %param.19, s32[]{:T(128)S(6)} %select_n.26), kind=kOutput, calls=%fused_computation.63 | convolution fusion | flops 4229116 | bytes 1077284 | tf_op jit(solution)/shard_map/dot_general | solution.py:106
  7.5 3.5 %fusion.50 = f32[4,32,2048]{2,1,0:T(8,128)S(1)} fusion(bf16[4,32,256]{2,1,0:T(8,128)(2,1)} %param.23, bf16[4,2048,256]{2,1,0:T(8,128)(2,1)} %param.20), kind=kOutput, calls=%fused_computation.101 | convolution fusion | flops 134217728 | bytes 5308416 | tf_op jit(solution)/shard_map/shc,spc->shp/dot_general | solution.py:116
  12.6 1.5 %copy.59 = bf16[256,2048]{0,1:T(8,128)(2,1)S(1)} copy(bf16[256,2048]{1,0:T(8,128)(2,1)} %param.29) | data formatting | bytes 2097152 | tf_op args[10]
  14.1 3.0 %fusion.5 = bf16[4,32,256]{2,1,0:T(8,128)(2,1)S(1)} fusion(bf16[4,2048,256]{2,1,0:T(8,128)(2,1)} %param.20, f32[4,32,2048]{2,1,0:T(8,128)S(1)} %get-tuple-element.14, f32[4,32]{1,0:T(4,128)S(1)} %get-tuple-element.8, f32[4,32]{1,0:T(4,128)S(1)} %fusion.39, f32[4,256]{1,0:T(4,128)S(1)} %get-tuple-element.3, f32[4,32]{1,0:T(4,128)S(1)} %get-tuple-element.7), kind=kOutput, calls=%fused_computation.10 | convolution fusion | flops 135102464 | bytes 5314048 | tf_op jit(solution)/shard_map/shp,spc->shc/dot_general | solution.py:134
  17.6 0.7 broadcast_in_dim.25
  18.3 6.4 %all-to-all-start = ((bf16[8,4,2048]{2,1,0:T(4,128)(2,1)}), bf16[8,4,2048]{2,1,0:T(4,128)(2,1)S(1)}, u32[]{:S(2)}, u32[]{:S(2)}) async-start(bf16[8,4,2048]{2,1,0:T(4,128)(2,1)} %broadcast_in_dim.25), calls=%async_computation | async-start | bytes 262144 | tf_op jit(solution)/shard_map/all_to_all | solution.py:56
  24.7 2.3 %copy.62 = bf16[256,2048]{0,1:T(8,128)(2,1)} copy(bf16[256,2048]{1,0:T(8,128)(2,1)} %param.30) | data formatting | bytes 2097152 | tf_op args[11]
  27.0 4.5 %all-to-all-done = bf16[8,4,2048]{2,1,0:T(4,128)(2,1)S(1)} async-done(((bf16[8,4,2048]{2,1,0:T(4,128)(2,1)}), bf16[8,4,2048]{2,1,0:T(4,128)(2,1)S(1)}, u32[]{:S(2)}, u32[]{:S(2)}) %all-to-all-start) | async-done | bytes 131104 | tf_op jit(solution)/shard_map/all_to_all | solution.py:56
  31.5 3.6 %all-to-all-start.1 = ((bf16[256,8,256]{0,2,1:T(8,128)(2,1)}), bf16[256,8,256]{0,2,1:T(8,128)(2,1)S(1)}, u32[]{:S(2)}, u32[]{:S(2)}) async-start(bf16[256,8,256]{0,2,1:T(8,128)(2,1)} %bitcast.8), calls=%async_computation.1 | async-start | bytes 2097152 | tf_op jit(solution)/shard_map/all_to_all | solution.py:155
  35.4 26.1 %all-to-all-done.1 = bf16[256,8,256]{0,2,1:T(8,128)(2,1)S(1)} async-done(((bf16[256,8,256]{0,2,1:T(8,128)(2,1)}), bf16[256,8,256]{0,2,1:T(8,128)(2,1)S(1)}, u32[]{:S(2)}, u32[]{:S(2)}) %all-to-all-start.1) | async-done | bytes 1048608 | tf_op jit(solution)/shard_map/all_to_all | solution.py:155
  62.0 1.0 fusion.8
  63.2 0.7 broadcast_in_dim.27
  63.9 3.5 %all-to-all-start.2 = ((bf16[32,16,256]{2,1,0:T(8,128)(2,1)}), bf16[32,16,256]{2,1,0:T(8,128)(2,1)S(1)}, u32[]{:S(2)}, u32[]{:S(2)}) async-start(bf16[32,16,256]{2,1,0:T(8,128)(2,1)} %bitcast.15), calls=%async_computation.2 | async-start | bytes 524288 | tf_op jit(solution)/shard_map/all_to_all | solution.py:181
  67.6 9.8 %all-to-all-done.2 = bf16[32,16,256]{2,1,0:T(8,128)(2,1)S(1)} async-done(((bf16[32,16,256]{2,1,0:T(8,128)(2,1)}), bf16[32,16,256]{2,1,0:T(8,128)(2,1)S(1)}, u32[]{:S(2)}, u32[]{:S(2)}) %all-to-all-start.2) | async-done | bytes 262176 | tf_op jit(solution)/shard_map/all_to_all | solution.py:181
  78.4 3.0 %convolution_bitcast_fusion.1 = f32[2,64,512]{2,1,0:T(8,128)S(1)} fusion(bf16[2,2048,512]{2,1,0:T(8,128)(2,1)} %param.35, bf16[64,2048]{1,0:T(8,128)(2,1)S(1)} %multiply_convert_fusion), kind=kOutput, calls=%fused_computation.7 | convolution fusion | flops 268435456 | bytes 4718592 | tf_op jit(solution)/shard_map/rd,edf->erf/dot_general | solution.py:196
  82.0 5.0 %fusion.2 = bf16[64,2048]{1,0:T(8,128)(2,1)S(1)} fusion(bf16[2,512,2048]{2,1,0:T(8,128)(2,1)} %param.37, bf16[2,2048,512]{2,1,0:T(8,128)(2,1)} %param.36, f32[2,64]{1,0:T(2,128)S(1)} %bitcast.112, bf16[64,2048]{1,0:T(8,128)(2,1)S(1)} %multiply_convert_fusion, f32[2,64,512]{2,1,0:T(8,128)S(1)} %convolution_bitcast_fusion.1), kind=kOutput, calls=%fused_computation.4 | convolution fusion | flops 537657344 | bytes 9175552 | tf_op jit(solution)/shard_map/erf,efd->erd/dot_general | solution.py:199
  87.2 12.7 %all_to_all.39 = bf16[32,16,256]{2,1,0:T(8,128)(2,1)S(1)} all-to-all(bf16[32,16,256]{2,1,0:T(8,128)(2,1)S(1)} %bitcast.100), channel_id=1, replica_groups=mesh['ep'=4,'tp'=8] {'ep','tp'}, dimensions={0} | all-to-all | bytes 524288 | tf_op jit(solution)/shard_map/all_to_all | solution.py:203
  100.8 3.4 %all-to-all-start.4 = ((bf16[8,32,256]{2,1,0:T(8,128)(2,1)}), bf16[8,32,256]{2,1,0:T(8,128)(2,1)S(1)}, u32[]{:S(2)}, u32[]{:S(2)}) async-start(bf16[8,32,256]{2,1,0:T(8,128)(2,1)} %broadcast_in_dim.28), calls=%async_computation.4 | async-start | bytes 262144 | tf_op jit(solution)/shard_map/all_to_all | solution.py:56
  104.8 6.0 %all-to-all-done.4 = bf16[8,32,256]{2,1,0:T(8,128)(2,1)S(1)} async-done(((bf16[8,32,256]{2,1,0:T(8,128)(2,1)}), bf16[8,32,256]{2,1,0:T(8,128)(2,1)S(1)}, u32[]{:S(2)}, u32[]{:S(2)}) %all-to-all-start.4) | async-done | bytes 131104 | tf_op jit(solution)/shard_map/all_to_all | solution.py:56
  (69 shorter events, 8.3 us)
Async XLA Ops:
  0.6 5.1 %copy-start = (bf16[2048,256]{1,0:T(8,128)(2,1)S(1)}, bf16[2048,256]{1,0:T(8,128)(2,1)}, u32[]{:S(2)}) copy-start(bf16[2048,256]{1,0:T(8,128)(2,1)} %param.26) | copy-start | bytes 3145732
  0.6 10.5 %copy-start.2 = (bf16[4,32,256]{2,1,0:T(8,128)(2,1)S(1)}, bf16[4,32,256]{2,1,0:T(8,128)(2,1)}, u32[]{:S(2)}) copy-start(bf16[4,32,256]{2,1,0:T(8,128)(2,1)} %param.23) | copy-start | bytes 196612
  0.7 11.1 %copy-start.1 = (bf16[4,32,2048]{2,1,0:T(8,128)(2,1)S(1)}, bf16[4,32,2048]{2,1,0:T(8,128)(2,1)}, u32[]{:S(2)}) copy-start(bf16[4,32,2048]{2,1,0:T(8,128)(2,1)} %param.21) | copy-start | bytes 1572868
  11.2 6.0 %copy-start.6 = (bf16[4,256]{1,0:T(4,128)(2,1)}, bf16[4,256]{1,0:T(4,128)(2,1)S(1)}, u32[]{:S(2)}) copy-start(bf16[4,256]{1,0:T(4,128)(2,1)S(1)} %get-tuple-element.4) | copy-start | bytes 6148
  17.1 18.0 %copy-start.7 = (s32[32,2]{0,1:T(2,128)S(1)}, s32[32,2]{0,1:T(2,128)}, u32[]{:S(2)}) copy-start(s32[32,2]{0,1:T(2,128)} %param.34) | copy-start | bytes 772
  18.3 13.1 %all-to-all-start = ((bf16[8,4,2048]{2,1,0:T(4,128)(2,1)}), bf16[8,4,2048]{2,1,0:T(4,128)(2,1)S(1)}, u32[]{:S(2)}, u32[]{:S(2)}) async-start(bf16[8,4,2048]{2,1,0:T(4,128)(2,1)} %broadcast_in_dim.25), calls=%async_computation | async-start | bytes 262144 | tf_op jit(solution)/shard_map/all_to_all | solution.py:56
  24.7 42.9 %copy-start.5 = (bf16[2048]{0:T(1024)(128)(2,1)S(1)}, bf16[2048]{0:T(1024)(128)(2,1)}, u32[]{:S(2)}) copy-start(bf16[2048]{0:T(1024)(128)(2,1)} %param.31) | copy-start | bytes 12292
  31.5 30.1 %all-to-all-start.1 = ((bf16[256,8,256]{0,2,1:T(8,128)(2,1)}), bf16[256,8,256]{0,2,1:T(8,128)(2,1)S(1)}, u32[]{:S(2)}, u32[]{:S(2)}) async-start(bf16[256,8,256]{0,2,1:T(8,128)(2,1)} %bitcast.8), calls=%async_computation.1 | async-start | bytes 2097152 | tf_op jit(solution)/shard_map/all_to_all | solution.py:155
  63.9 13.5 %all-to-all-start.2 = ((bf16[32,16,256]{2,1,0:T(8,128)(2,1)}), bf16[32,16,256]{2,1,0:T(8,128)(2,1)S(1)}, u32[]{:S(2)}, u32[]{:S(2)}) async-start(bf16[32,16,256]{2,1,0:T(8,128)(2,1)} %bitcast.15), calls=%async_computation.2 | async-start | bytes 524288 | tf_op jit(solution)/shard_map/all_to_all | solution.py:181
  77.5 3.9 %copy-start.4 = (bf16[2048,4]{0,1:T(4,128)(2,1)S(1)}, bf16[2048,4]{0,1:T(4,128)(2,1)}, u32[]{:S(2)}) copy-start(bf16[2048,4]{0,1:T(4,128)(2,1)} %param.32) | copy-start | bytes 49156
  77.5 4.1 %copy-start.3 = (bf16[2048,8]{0,1:T(8,128)(2,1)S(1)}, bf16[2048,8]{0,1:T(8,128)(2,1)}, u32[]{:S(2)}) copy-start(bf16[2048,8]{0,1:T(8,128)(2,1)} %param.33) | copy-start | bytes 98308
  100.8 10.1 %all-to-all-start.4 = ((bf16[8,32,256]{2,1,0:T(8,128)(2,1)}), bf16[8,32,256]{2,1,0:T(8,128)(2,1)S(1)}, u32[]{:S(2)}, u32[]{:S(2)}) async-start(bf16[8,32,256]{2,1,0:T(8,128)(2,1)} %broadcast_in_dim.28), calls=%async_computation.4 | async-start | bytes 262144 | tf_op jit(solution)/shard_map/all_to_all | solution.py:56

commit v2 on v0

v2 whole, which is shorter than its diff:
```python
import functools

import jax
import jax.numpy as jnp
from jax import lax
from jax.experimental import pallas as pl
from jax.experimental.pallas import tpu as pltpu
from jax.sharding import PartitionSpec as P

H = 32
KV = 256
ROPE = 32
NOPE = 64
V = 64
GROUPS = 4
TOPK = 2


NORM_EPSILON = 1e-06
ROPE_BASE = 10000.0
F32 = jnp.float32
BF16 = jnp.bfloat16
VMEM = pl.BlockSpec(memory_space=pltpu.VMEM)
SMEM = pl.BlockSpec(memory_space=pltpu.SMEM)
HBM = pl.BlockSpec(memory_space=pltpu.HBM)


def inverse_rms(values):
    return lax.rsqrt(jnp.mean(values * values, axis=-1, keepdims=True) + NORM_EPSILON)


def iota(shape, dim):
    return lax.broadcasted_iota(jnp.int32, shape, dim)


def dot(a, b, dims=((1,), (0,)), precision=None):
    return lax.dot_general(a, b, (dims, ((), ())), precision=precision, preferred_element_type=F32)


NT = ((1,), (1,))


def attention_kernel(
    lengths,
    residual_hbm,
    query_latent_hbm,
    query_rope_hbm,
    norm_gain_hbm,
    latent_gain_hbm,
    rope_weight_hbm,
    latent_weight_hbm,
    value_weight_hbm,
    cache_latent_hbm,
    cache_rope_hbm,
    heads_out,
    new_latent_out,
    new_rope_out,
    residual,
    query_latent,
    query_rope,
    norm_gain,
    latent_gain,
    rope_weight,
    latent_weight,
    value_weight,
    cache_latent,
    cache_rope,
    mixed,
    head_rows,
    sems,
):
    seqs = cache_latent.shape[0]
    rows = residual.shape[0]
    loads = []

    def load(source, target):
        copy = pltpu.make_async_copy(source, target, sems.at[len(loads)])
        loads.append(copy)
        copy.start()
        return copy

    latent_loads, rope_loads = [], []
    own_loads = [
        load(residual_hbm, residual),
        load(norm_gain_hbm, norm_gain),
        load(rope_weight_hbm, rope_weight),
        load(latent_gain_hbm, latent_gain),
        load(query_latent_hbm, query_latent),
        load(query_rope_hbm, query_rope),
    ]
    weight_load = load(latent_weight_hbm, latent_weight)
    for s in range(seqs):
        latent_loads.append(load(cache_latent_hbm.at[s], cache_latent.at[s]))
        rope_loads.append(load(cache_rope_hbm.at[s], cache_rope.at[s]))
    value_load = load(value_weight_hbm, value_weight)

    lane = iota((1, ROPE), 1)
    half = ROPE // 2
    low = lane < half
    step = jnp.where(low, lane, lane - half)
    frequency = jnp.zeros((1, ROPE), F32)
    for i in range(half):
        frequency = jnp.where(step == i, F32(ROPE_BASE ** (-2.0 * i / ROPE)), frequency)
    seq_row = iota((seqs, ROPE), 0)
    position = jnp.zeros((seqs, ROPE), F32)
    for s in range(seqs):
        position = jnp.where(seq_row == s, lengths[s].astype(F32), position)
    angles = position * frequency
    cosine = jnp.cos(angles)
    sine = jnp.sin(angles) * jnp.where(low, F32(-1), F32(1))

    for copy in own_loads:
        copy.wait()
    first = lax.axis_index("tp") * seqs
    own_pick = (iota((seqs, rows), 1) == iota((seqs, rows), 0) + first).astype(BF16)
    own = dot(own_pick, residual[...])
    normed = (own * inverse_rms(own) * norm_gain[...].astype(F32)[None, :]).astype(BF16)
    rope_rows = rope_weight[...]
    rope_swapped = jnp.concatenate([rope_rows[half:], rope_rows[:half]], axis=0)
    rope_key = dot(normed, rope_rows, NT) * cosine + dot(normed, rope_swapped, NT) * sine
    rope_key = rope_key.astype(BF16)
    new_rope_out[...] = rope_key
    weight_load.wait()
    latent_raw = dot(normed, latent_weight[...])
    new_latent = latent_raw * inverse_rms(latent_raw) * latent_gain[...].astype(F32)[None, :]
    new_latent = new_latent.astype(BF16)
    new_latent_out[...] = new_latent

    swap = (iota((ROPE, ROPE), 0) == (iota((ROPE, ROPE), 1) + half) % ROPE).astype(BF16)
    scale = (NOPE + ROPE) ** (-0.5)
    for s in range(seqs):
        turning = query_rope[s]
        turned = turning.astype(F32) * cosine[s : s + 1] + dot(turning, swap) * sine[s : s + 1]
        turned = turned.astype(BF16)
        query = query_latent[s]
        fresh_latent = new_latent[s : s + 1].astype(F32)
        fresh_rope = rope_key[s : s + 1].astype(F32)
        fresh = (
            jnp.sum(query.astype(F32) * fresh_latent, axis=1, keepdims=True)
            + jnp.sum(turned.astype(F32) * fresh_rope, axis=1, keepdims=True)
        ) * scale
        latent_loads[s].wait()
        score = dot(query, cache_latent[s], NT)
        rope_loads[s].wait()
        score = (score + dot(turned, cache_rope[s])) * scale
        score = jnp.where(iota(score.shape, 1) < lengths[s], score, -jnp.inf)
        top = jnp.maximum(jnp.max(score, axis=1, keepdims=True), fresh)
        score = jnp.exp(score - top)
        fresh = jnp.exp(fresh - top)
        share = 1.0 / (jnp.sum(score, axis=1, keepdims=True) + fresh)
        weight = (score * share).astype(BF16)
        fresh = (fresh * share).astype(BF16).astype(F32)
        mix = dot(weight, cache_latent[s]) + fresh * fresh_latent
        mixed[s * H : (s + 1) * H, :] = mix.astype(BF16)

    value_load.wait()
    spread = dot(mixed[...], value_weight[...])
    first = iota((H, H * V), 0) * V
    column = iota((H, H * V), 1)
    own_head = (column >= first) & (column < first + V)
    for s in range(seqs):
        kept = jnp.where(own_head, spread[s * H : (s + 1) * H], F32(0))
        head_rows[s : s + 1, :] = jnp.sum(kept, axis=0, keepdims=True)
    shares, _, width = heads_out.shape
    for t in range(shares):
        heads_out[t] = head_rows[:, t * width : (t + 1) * width].astype(BF16)


def attention(
    lengths, residual, query_latent, query_rope, norm_gain, latent_gain, rope_weight,
    latent_weight, value_weight, cache_latent, cache_rope, shares,
):
    seqs, cached, _ = cache_latent.shape
    width = H * V // shares
    return pl.pallas_call(
        attention_kernel,
        name="attention",
        out_shape=(
            jax.ShapeDtypeStruct((shares, seqs, width), BF16),
            jax.ShapeDtypeStruct((seqs, KV), BF16),
            jax.ShapeDtypeStruct((seqs, ROPE), BF16),
        ),
        in_specs=[SMEM] + [HBM] * 10,
        out_specs=(VMEM, VMEM, VMEM),
        scratch_shapes=[
            pltpu.VMEM(residual.shape, BF16),
            pltpu.VMEM(query_latent.shape, BF16),
            pltpu.VMEM(query_rope.shape, BF16),
            pltpu.VMEM(norm_gain.shape, BF16),
            pltpu.VMEM(latent_gain.shape, BF16),
            pltpu.VMEM(rope_weight.shape, BF16),
            pltpu.VMEM(latent_weight.shape, BF16),
            pltpu.VMEM(value_weight.shape, BF16),
            pltpu.VMEM(cache_latent.shape, BF16),
            pltpu.VMEM(cache_rope.shape, BF16),
            pltpu.VMEM((seqs * H, KV), BF16),
            pltpu.VMEM((seqs, H * V), F32),
            pltpu.SemaphoreType.DMA((2 * seqs + 8,)),
        ],
        cost_estimate=pl.CostEstimate(
            flops=2 * seqs * H * cached * (2 * KV + ROPE), bytes_accessed=8 * 2**20, transcendentals=0
        ),
    )(
        lengths, residual, query_latent, query_rope, norm_gain, latent_gain, rope_weight,
        latent_weight, value_weight, cache_latent, cache_rope,
    )


def project_kernel(heads, out_weight, terms_out, gathered):
    shares, seqs, _ = heads.shape
    for t in range(shares):
        gathered[t * seqs : (t + 1) * seqs, :] = heads[t].astype(F32)
    terms = dot(gathered[...].astype(BF16), out_weight[...])
    width = terms_out.shape[2]
    for t in range(shares):
        terms_out[t] = terms[:, t * width : (t + 1) * width].astype(BF16)


def project(heads, out_weight):
    shares, seqs, width = heads.shape
    columns = out_weight.shape[1]
    return pl.pallas_call(
        project_kernel,
        name="project",
        out_shape=jax.ShapeDtypeStruct((shares, shares * seqs, columns // shares), BF16),
        in_specs=[VMEM, VMEM],
        out_specs=VMEM,
        scratch_shapes=[pltpu.VMEM((shares * seqs, width), F32)],
        compiler_params=pltpu.CompilerParams(vmem_limit_bytes=8 * 2**20),
        cost_estimate=pl.CostEstimate(
            flops=2 * shares * seqs * width * columns, bytes_accessed=2**20, transcendentals=0
        ),
    )(heads, out_weight)


def dispatch_kernel(local_experts, slots, terms, residual, expert_ids, sent_out, after_out, pick_out):
    shares, rows, width = terms.shape
    total = terms[0].astype(F32)
    for t in range(1, shares):
        total = total + terms[t].astype(F32)
    first = pl.multiple_of(lax.axis_index("tp") * width, width)
    ep_count = sent_out.shape[0] // shares
    after = (residual[:, pl.ds(first, width)].astype(F32) + total).astype(BF16)
    after_out[...] = after

    index = iota((ep_count, rows), 0) * local_experts
    hit = None
    for k in range(TOPK):
        named = expert_ids[k : k + 1, :]
        here = (named >= index) & (named < index + local_experts)
        hit = here if hit is None else hit | here
    hit = hit.astype(F32)
    earlier = (iota((rows, rows), 0) < iota((rows, rows), 1)).astype(BF16)
    rank = dot(hit.astype(BF16), earlier)
    rank = jnp.where(hit > 0.5, rank, F32(-1))
    slot = iota((slots, rows), 0).astype(F32)
    for e in range(ep_count):
        pick = (rank[e : e + 1, :] == slot).astype(F32)
        pick_out[e * slots : (e + 1) * slots, :] = pick
    chosen = dot(pick_out[...].astype(BF16), after).astype(BF16)
    for e in range(ep_count):
        for t in range(shares):
            sent_out[e * shares + t] = chosen[e * slots : (e + 1) * slots]


def dispatch(terms, residual, expert_ids, ep_count, local_experts, slots):
    shares, rows, width = terms.shape
    return pl.pallas_call(
        functools.partial(dispatch_kernel, local_experts, slots),
        name="dispatch",
        out_shape=(
            jax.ShapeDtypeStruct((ep_count * shares, slots, width), BF16),
            jax.ShapeDtypeStruct((rows, width), BF16),
            jax.ShapeDtypeStruct((ep_count * slots, rows), F32),
        ),
        in_specs=[VMEM] * 3,
        out_specs=(VMEM, VMEM, VMEM),
        compiler_params=pltpu.CompilerParams(vmem_limit_bytes=8 * 2**20),
        cost_estimate=pl.CostEstimate(flops=10**6, bytes_accessed=2**20, transcendentals=0),
    )(terms, residual, expert_ids)


def experts_kernel(
    shares, came, mixer_gain, group_router, expert_router, choice, gate_hbm, up_hbm, down_hbm,
    back_out, rows_in, gate, up, down, sems,
):
    loads = []
    for l in range(gate.shape[0]):
        for n, (source, target) in enumerate(((gate_hbm, gate), (up_hbm, up), (down_hbm, down))):
            copy = pltpu.make_async_copy(source.at[l], target.at[l], sems.at[3 * l + n])
            copy.start()
            loads.append(copy)
    ep_count = came.shape[0] // shares
    _, slots, width = came.shape
    for e in range(ep_count):
        for t in range(shares):
            rows_in[e * slots : (e + 1) * slots, t * width : (t + 1) * width] = came[e * shares + t]
    after = rows_in[...].astype(F32)
    expert_in = (after * inverse_rms(after) * mixer_gain[...].astype(F32)[None, :]).astype(BF16)

    group_logits = dot(expert_in, group_router[...], NT)
    expert_logits = dot(expert_in, expert_router[...], NT)
    choices = choice[...]
    group_hit = iota(group_logits.shape, 1) == choices[:, 2 * TOPK : 2 * TOPK + 1]
    own_group = jnp.sum(jnp.where(group_hit, group_logits, F32(0)), axis=1, keepdims=True)
    group_share = 1.0 / jnp.sum(jnp.exp(group_logits - own_group), axis=1, keepdims=True)
    picked = []
    for k in range(TOPK):
        expert_hit = iota(expert_logits.shape, 1) == choices[:, k : k + 1]
        picked.append(jnp.sum(jnp.where(expert_hit, expert_logits, F32(0)), axis=1, keepdims=True))
    route = []
    for k in range(TOPK):
        total = jnp.exp(picked[0] - picked[k])
        for j in range(1, TOPK):
            total = total + jnp.exp(picked[j] - picked[k])
        route.append(group_share / total)

    result = None
    for l in range(gate.shape[0]):
        weight = jnp.where(choices[:, TOPK : TOPK + 1] == l, route[0], F32(0))
        for k in range(1, TOPK):
            weight = weight + jnp.where(choices[:, TOPK + k : TOPK + k + 1] == l, route[k], F32(0))
        loads[3 * l].wait()
        gated = dot(expert_in, gate[l])
        loads[3 * l + 1].wait()
        raised = dot(expert_in, up[l])
        act = (gated / (1.0 + jnp.exp(-gated)) * raised).astype(BF16)
        loads[3 * l + 2].wait()
        part = dot(act, down[l]) * weight
        result = part if result is None else result + part
    result = result.astype(BF16)
    for e in range(ep_count):
        for t in range(shares):
            back_out[e * shares + t] = result[e * slots : (e + 1) * slots, t * width : (t + 1) * width]


def run_experts(came, mixer_gain, group_router, expert_router, choice, gate, up, down, shares):
    count, slots, width = came.shape
    rows, model = count // shares * slots, shares * width
    return pl.pallas_call(
        functools.partial(experts_kernel, shares),
        name="experts",
        out_shape=jax.ShapeDtypeStruct(came.shape, BF16),
        in_specs=[VMEM] * 5 + [HBM] * 3,
        out_specs=VMEM,
        scratch_shapes=[
            pltpu.VMEM((rows, model), BF16),
            pltpu.VMEM(gate.shape, BF16),
            pltpu.VMEM(up.shape, BF16),
            pltpu.VMEM(down.shape, BF16),
            pltpu.SemaphoreType.DMA((3 * gate.shape[0],)),
        ],
        cost_estimate=pl.CostEstimate(
            flops=6 * rows * gate.size, bytes_accessed=6 * gate.size, transcendentals=0
        ),
    )(came, mixer_gain, group_router, expert_router, choice, gate, up, down)


def combine_kernel(shares, back, pick, after, copies_out, sums):
    count, slots, _ = back.shape
    for e in range(count // shares):
        total = back[e * shares].astype(F32)
        for t in range(1, shares):
            total = total + back[e * shares + t].astype(F32)
        sums[e * slots : (e + 1) * slots, :] = total
    moe = dot(pick[...], sums[...], ((0,), (0,)), lax.Precision.HIGHEST)
    mixed = (after[...].astype(F32) + moe).astype(BF16)
    for t in range(shares):
        copies_out[t] = mixed


def combine(back, pick, after, shares):
    count, slots, width = back.shape
    return pl.pallas_call(
        functools.partial(combine_kernel, shares),
        name="combine",
        out_shape=jax.ShapeDtypeStruct((shares,) + after.shape, BF16),
        in_specs=[VMEM] * 3,
        out_specs=VMEM,
        scratch_shapes=[pltpu.VMEM((count // shares * slots, width), F32)],
        compiler_params=pltpu.CompilerParams(vmem_limit_bytes=8 * 2**20),
        cost_estimate=pl.CostEstimate(flops=10**6, bytes_accessed=2**20, transcendentals=0),
    )(back, pick, after)


def exchange(blocks, axis):
    return lax.all_to_all(blocks, axis, split_axis=0, concat_axis=0, tiled=True)


def slot_owners(expert_ids, local_experts):
    return (expert_ids // local_experts).T


def slot_table(owners, index, slots):
    hit = jnp.any(owners == index, axis=0).astype(jnp.int32)
    rank = jnp.cumsum(hit) - hit
    return (rank[None, :] == jnp.arange(slots)[:, None]) & (hit[None, :] > 0)


def on_device(
    residual,
    cache_latent,
    cache_rope,
    lengths,
    query_latent,
    query_rope,
    norm_gain,
    latent_weight,
    latent_gain,
    rope_weight,
    value_weight,
    out_weight,
    mixer_gain,
    group_router,
    expert_router,
    expert_ids,
    gate_weight,
    up_weight,
    down_weight,
):
    ep_count = lax.axis_size("ep")
    tp_count = lax.axis_size("tp")
    group_rows, model_width = residual.shape
    experts = expert_router.shape[1]
    per_group = experts // GROUPS
    local_experts = gate_weight.shape[0]
    capacity = 2 * group_rows * TOPK // experts
    whole_groups = per_group == TOPK and local_experts == TOPK
    slots = capacity if whole_groups else capacity * local_experts
    first_expert = lax.axis_index("ep") * local_experts
    if whole_groups:
        slot_ids = jnp.broadcast_to(
            first_expert + jnp.arange(TOPK, dtype=jnp.int32)[None], (ep_count * slots, TOPK)
        )
    else:
        all_ids = lax.all_gather(expert_ids, "ep")
        mine = jax.vmap(
            lambda ids: slot_table(slot_owners(ids, local_experts), lax.axis_index("ep"), slots)
        )(all_ids)
        slot_ids = jnp.sum(
            mine[:, :, :, None].astype(jnp.int32) * all_ids[:, None, :, :], axis=2
        ).reshape(-1, TOPK)
    choice = jnp.concatenate(
        [slot_ids, slot_ids - first_expert, slot_ids[:, :1] // per_group], axis=1
    )

    heads, new_latent, new_rope_key = attention(
        lengths, residual, query_latent, query_rope, norm_gain, latent_gain,
        rope_weight, latent_weight, value_weight, cache_latent, cache_rope, tp_count,
    )
    terms = project(exchange(heads, "tp"), out_weight)
    sent, after, pick = dispatch(
        exchange(terms, "tp"), residual, expert_ids.T, ep_count, local_experts, slots
    )
    back = run_experts(
        exchange(sent, ("ep", "tp")), mixer_gain, group_router.T, expert_router.T, choice,
        gate_weight, up_weight, down_weight, tp_count,
    )
    copies = combine(exchange(back, ("ep", "tp")), pick, after, tp_count)
    mixed = exchange(copies, "tp").transpose(1, 0, 2).reshape(group_rows, model_width)
    return (mixed, new_latent, new_rope_key)


def solution(mesh):
    in_specs = (
        P("ep", None),
        P(("ep", "tp"), None, None),
        P(("ep", "tp"), None, None),
        P(("ep", "tp")),
        P(("ep", "tp"), None, None),
        P(("ep", "tp"), None, None),
        P(),
        P(),
        P(),
        P(),
        P(),
        P("tp", None),
        P(),
        P(),
        P(),
        P("ep", None),
        P("ep", None, "tp"),
        P("ep", None, "tp"),
        P("ep", "tp", None),
    )
    out_specs = (P("ep", None), P(("ep", "tp"), None), P(("ep", "tp"), None))
    return jax.shard_map(
        on_device, mesh=mesh, in_specs=in_specs, out_specs=out_specs, check_vma=False
    )
```

time: 178 us -> 77.6 us (0.44)
  waiting for transfers between devices: 93.9 us -> 8.95 us
  matrix products: 21.4 us -> 0 us
  blocking collectives: 24.5 us -> 43.5 us
  Pallas kernels: 0 us -> 18 us
  between operations: 14.3 us -> 0.87 us
  other arithmetic: 7.81 us -> 0.08 us
  starting transfers between devices: 10.1 us -> 3.68 us
  local copies, waits for them, and re-layouts: 5.06 us -> 2.17 us
    psum x1 -> x0, waiting for transfers between devices: 53.8 us -> none  [on_device(): attended = lax.psum(head_terms, 'tp')]
    all_to_all x1 -> x4, blocking collectives: 10.6 us -> 43.5 us  [exchange(): return lax.all_to_all(blocks, axis, split_axis=0, concat_axis=0, tiled=True)]
    reduce_scatter x1 -> x0, waiting for transfers between devices: 30.9 us -> none  [on_device(): lax.psum_scatter(expert_terms, 'tp', scatter_dimension=3, tiled=True)]
    dot_general x15 -> x0, matrix products: 21.4 us -> none  [the longest x1 6.04 us: on_device(): jnp.einsum('secf,efd->secd', activation, down_weight, preferred_element_t...]
    pallas_call x0 -> x5, Pallas kernels: none -> 18 us  [the longest x1 9.62 us: attention(): pl.pallas_call(attention_kernel, name='attention', out_shape=(jax.ShapeDt...]
    all_gather x1 -> x0, blocking collectives: 14 us -> none  [on_device(): mixed = lax.all_gather(mixed_share, 'tp', axis=1, tiled=True)]
    all_to_all x2 -> x1, starting transfers between devices: 10 us -> 3.68 us  [exchange(): return lax.all_to_all(blocks, axis, split_axis=0, concat_axis=0, tiled=True)]
    convert_element_type x10 -> x0, other arithmetic: 4.1 us -> none  [the longest x1 0.93 us: on_device(): resid_f = residual.astype(jnp.float32)]
  transfers between devices with their start and end apart: 4 -> 1, of which waited for: 4 -> 1; matrix products, arithmetic and copies ran while one was open for 1% -> 1% of each run, Pallas kernels for 0% -> 0%
where the time goes in v2:
time: 77.6 us; the launch traced here: 77.2 us
  blocking collectives  43.5 us (56%)
  Pallas kernels  18 us (23%)
  waiting for transfers between devices  8.95 us (12%)
  starting transfers between devices  3.68 us (5%)
  local copies, waits for them, and re-layouts  2.17 us (3%)
  between operations  0.87 us (1%)
    all_to_all x4, blocking collectives, exchange(): return lax.all_to_all(blocks, axis, split_axis=0, concat_axis=0, tiled=True)  43.5 us
    pallas_call x1, Pallas kernels, attention(): pl.pallas_call(attention_kernel, name='attention', out_shape=(jax.ShapeDt...  9.62 us
    all_to_all x1, waiting for transfers between devices, exchange(): return lax.all_to_all(blocks, axis, split_axis=0, concat_axis=0, tiled=True)  8.95 us
    pallas_call x1, Pallas kernels, run_experts(): pl.pallas_call(functools.partial(experts_kernel, shares), name='experts',...  6.88 us
    all_to_all x1, starting transfers between devices, exchange(): return lax.all_to_all(blocks, axis, split_axis=0, concat_axis=0, tiled=True)  3.68 us
  transfers between devices with their start and end apart: 1, of which 1 were waited for; matrix products, arithmetic and copies ran while one was open for 1% of the time, Pallas kernels for 0%

profile of v2, /device:TPU:0, one launch (start us, length us, event | category | flops | bytes accessed | tf_op | source)
XLA Modules:
  0.0 77.2 jit_solution(6289248068598602989)
XLA Ops:
  0.6 0.0 copy-start.1
  0.6 0.0 copy-start
  0.7 0.0 copy-start.2
  0.7 9.6 %attention.1 = (bf16[8,4,256]{2,1,0:T(4,128)(2,1)}, bf16[4,256]{1,0:T(4,128)(2,1)}, bf16[4,32]{1,0:T(4,128)(2,1)}) custom-call(s32[4]{0:T(128)} %lengths.1, bf16[32,2048]{1,0:T(8,128)(2,1)} %residual.1, bf16[4,32,256]{2,1,0:T(8,128)(2,1)} %query_latent_hbm.1, bf16[4,32,32]{2,1,0:T(8,128)(2,1)} %query_rope_hbm.1, bf16[2048]{0:T(1024)(128)(2,1)} %norm_gain_hbm.1, ...), custom_call_target="tpu_custom_call" | custom-call | flops 285212672 | bytes 8388608 | tf_op jit(solution)/shard_map/attention/pallas_call | solution.py:175
  10.3 12.0 %all_to_all.25.heads = bf16[8,4,256]{2,1,0:T(4,128)(2,1)S(1)} all-to-all(bf16[8,4,256]{2,1,0:T(4,128)(2,1)} %get-tuple-element.9), channel_id=1, replica_groups=mesh['ep'=4,'tp'=8] {'tp'}, dimensions={0} | all-to-all | bytes 32768 | tf_op jit(solution)/shard_map/all_to_all | solution.py:387
  22.3 0.0 copy-done
  22.3 0.3 project.1
  22.6 9.1 %all_to_all.26.terms = bf16[8,32,256]{2,1,0:T(8,128)(2,1)S(1)} all-to-all(bf16[8,32,256]{2,1,0:T(8,128)(2,1)S(1)} %project.1), channel_id=1, replica_groups=mesh['ep'=4,'tp'=8] {'tp'}, dimensions={0} | all-to-all | bytes 262144 | tf_op jit(solution)/shard_map/all_to_all | solution.py:387
  31.7 0.0 copy-done.1
  31.7 0.0 copy-done.2
  31.7 1.0 %dispatch.1 = (bf16[32,16,256]{2,1,0:T(8,128)(2,1)}, bf16[32,256]{1,0:T(8,128)(2,1)S(1)}, f32[64,32]{1,0:T(8,128)S(1)}) custom-call(bf16[8,32,256]{2,1,0:T(8,128)(2,1)S(1)} %all_to_all.26.terms, bf16[32,2048]{1,0:T(8,128)(2,1)S(1)} %copy-done.1, s32[2,32]{1,0:T(2,128)S(1)} %bitcast.9), custom_call_target="tpu_custom_call" | custom-call | flops 1000000 | bytes 1048576 | tf_op jit(solution)/shard_map/dispatch/pallas_call | solution.py:268
  32.7 3.7 %all-to-all-start.2 = ((bf16[32,16,256]{2,1,0:T(8,128)(2,1)}), bf16[32,16,256]{2,1,0:T(8,128)(2,1)S(1)}, u32[]{:S(2)}, u32[]{:S(2)}) async-start(bf16[32,16,256]{2,1,0:T(8,128)(2,1)} %get-tuple-element.10), calls=%async_computation.2 | async-start | bytes 524288 | tf_op jit(solution)/shard_map/all_to_all | solution.py:387
  36.6 0.1 pad.2.clone
  36.7 0.1 add_add_fusion
  36.7 0.7 copy.23.choice
  37.4 8.9 %all-to-all-done.2.came = bf16[32,16,256]{2,1,0:T(8,128)(2,1)S(1)} async-done(((bf16[32,16,256]{2,1,0:T(8,128)(2,1)}), bf16[32,16,256]{2,1,0:T(8,128)(2,1)S(1)}, u32[]{:S(2)}, u32[]{:S(2)}) %all-to-all-start.2) | async-done | bytes 262176 | tf_op jit(solution)/shard_map/all_to_all | solution.py:387
  46.4 0.0 copy-start.3
  46.4 0.7 copy-done.3
  47.1 6.9 %experts.1 = bf16[32,16,256]{2,1,0:T(8,128)(2,1)} custom-call(bf16[32,16,256]{2,1,0:T(8,128)(2,1)} %copy-done.3, bf16[2048]{0:T(1024)(128)(2,1)} %mixer_gain.1, bf16[4,2048]{1,0:T(4,128)(2,1)} %bitcast.13, bf16[8,2048]{1,0:T(8,128)(2,1)} %bitcast.12, s32[64,5]{1,0:T(8,128)} %copy.23.choice, bf16[2,2048,512]{2,1,0:T(8,128)(2,1)} %gate_hbm.1, ...), custom_call_target="tpu_custom_call" | custom-call | flops 805306368 | bytes 12582912 | tf_op jit(solution)/shard_map/experts/pallas_call | solution.py:340
  54.0 12.9 %all_to_all.27.back = bf16[32,16,256]{2,1,0:T(8,128)(2,1)S(1)} all-to-all(bf16[32,16,256]{2,1,0:T(8,128)(2,1)} %experts.1), channel_id=1, replica_groups=mesh['ep'=4,'tp'=8] {'ep','tp'}, dimensions={0} | all-to-all | bytes 524288 | tf_op jit(solution)/shard_map/all_to_all | solution.py:387
  66.9 0.2 combine.1
  67.1 9.4 %all_to_all.28 = bf16[8,32,256]{2,1,0:T(8,128)(2,1)S(1)} all-to-all(bf16[8,32,256]{2,1,0:T(8,128)(2,1)S(1)} %combine.1), channel_id=1, replica_groups=mesh['ep'=4,'tp'=8] {'tp'}, dimensions={0} | all-to-all | bytes 262144 | tf_op jit(solution)/shard_map/all_to_all | solution.py:387
  76.5 0.7 copy.25
  (4 shorter events, 0.0 us)
Async XLA Ops:
  0.6 31.1 %copy-start.1 = (bf16[32,2048]{1,0:T(8,128)(2,1)S(1)}, bf16[32,2048]{1,0:T(8,128)(2,1)}, u32[]{:S(2)}) copy-start(bf16[32,2048]{1,0:T(8,128)(2,1)} %residual.1) | copy-start | bytes 393220
  0.6 21.7 %copy-start = (bf16[256,2048]{1,0:T(8,128)(2,1)S(1)}, bf16[256,2048]{1,0:T(8,128)(2,1)}, u32[]{:S(2)}) copy-start(bf16[256,2048]{1,0:T(8,128)(2,1)} %out_weight.1) | copy-start | bytes 3145732
  0.7 31.1 %copy-start.2 = (s32[32,2]{0,1:T(2,128)S(1)}, s32[32,2]{0,1:T(2,128)}, u32[]{:S(2)}) copy-start(s32[32,2]{0,1:T(2,128)} %param.34) | copy-start | bytes 772
  32.7 13.7 %all-to-all-start.2 = ((bf16[32,16,256]{2,1,0:T(8,128)(2,1)}), bf16[32,16,256]{2,1,0:T(8,128)(2,1)S(1)}, u32[]{:S(2)}, u32[]{:S(2)}) async-start(bf16[32,16,256]{2,1,0:T(8,128)(2,1)} %get-tuple-element.10), calls=%async_computation.2 | async-start | bytes 524288 | tf_op jit(solution)/shard_map/all_to_all | solution.py:387
  46.4 0.7 copy-start.3
